TPU v7x, 32 devices: a whole 2x2x4 slice. The times are simulated.
32 devices in a mesh: sp: 2 (over x), dp: 16 (over z, y, core).
Axes of the slice: x: 2, y: 2, z: 4, core: 2. Of those that a mesh axis runs over, the one named last changes fastest.
Arguments:
- queries: bfloat16 [16, 384, 16, 128], P('dp', 'sp'), may hold values from -6 to 6
- keys: bfloat16 [16, 384, 16, 128], P('dp', 'sp'), may hold values from -6 to 6
- values: bfloat16 [16, 384, 16, 128], P('dp', 'sp'), may hold values from -6 to 6
- mix_ratio: float32 [16], replicated, may hold values from 0.3 to 0.8
- out_gain: float32 [128], replicated, may hold values from 0.1 to 1.9
- out_weight: bfloat16 [2048, 2048], P(None, 'dp'), may hold values from -0.125 to 0.125
Outputs:
- layer_out: bfloat16 [16, 384, 2048], P('dp', 'sp')
All inputs are finite; a program needn't handle non-finite values.
Results may differ from a plain program's by a relative error of at most 0.0098.
Values may be sent and summed in bfloat16 or wider, within the bound.
A program may use at most 64 MiB of HBM per device.

v0:
```python
import math
import jax
import jax.numpy as jnp
from jax import lax
from jax.sharding import PartitionSpec as P

theta_base = 500000.0
neg_large = -1e30
norm_eps = 1e-05


def rotate_halves(field, positions):
    width = field.shape[-1] // 2
    half = width // 2
    freqs = theta_base ** (-jnp.arange(half, dtype=jnp.float32) * 2.0 / width)
    angle = positions.astype(jnp.float32)[:, None] * freqs[None, :]
    cosine = jnp.cos(angle)[:, None, :]
    sine = jnp.sin(angle)[:, None, :]
    parts = field.reshape(field.shape[0], 2, width)
    lower = parts[..., :half]
    upper = parts[..., half:]
    turned = jnp.concatenate(
        [lower * cosine - upper * sine, upper * cosine + lower * sine], axis=-1
    )
    return turned.reshape(field.shape)


def masked_softmax(scores, visible):
    kept = jnp.where(visible, scores, neg_large)
    highest = jnp.max(kept, axis=-1, keepdims=True)
    powers = jnp.exp(kept - highest)
    return powers / jnp.sum(powers, axis=-1, keepdims=True)


def head_attention(query_head, key_head, value_head, ratio, gain):
    length = query_head.shape[0]
    width = query_head.shape[1] // 2
    positions = jnp.arange(length, dtype=jnp.int32)
    rotated_queries = (
        rotate_halves(query_head.astype(jnp.float32), positions) * width ** (-0.5)
    ).astype(jnp.bfloat16)
    rotated_keys = rotate_halves(key_head.astype(jnp.float32), positions).astype(jnp.bfloat16)
    block = math.gcd(512, length)

    def one_block(start):
        query_rows = lax.dynamic_slice_in_dim(rotated_queries, start, block, 0)
        visible = (start + jnp.arange(block, dtype=jnp.int32))[:, None] >= positions[None, :]
        first = jnp.dot(
            query_rows[:, :width], rotated_keys[:, :width].T, preferred_element_type=jnp.float32
        )
        second = jnp.dot(
            query_rows[:, width:], rotated_keys[:, width:].T, preferred_element_type=jnp.float32
        )
        weights = (masked_softmax(first, visible) - ratio * masked_softmax(second, visible)).astype(
            jnp.bfloat16
        )
        mixed = jnp.dot(weights, value_head, preferred_element_type=jnp.float32)
        scale = lax.rsqrt(jnp.mean(mixed * mixed, axis=-1, keepdims=True) + norm_eps)
        return (mixed * scale * gain).astype(jnp.bfloat16)

    starts = jnp.arange(length // block, dtype=jnp.int32) * block
    return lax.map(one_block, starts).reshape(length, value_head.shape[1])


def on_device(queries, keys, values, mix_ratio, out_gain, out_weight):
    groups = lax.axis_size("sp")
    heads_here = queries.shape[2] // groups
    query_all, key_all, value_all = (
        lax.all_to_all(queries, "sp", split_axis=2, concat_axis=1, tiled=True),
        lax.all_to_all(keys, "sp", split_axis=2, concat_axis=1, tiled=True),
        lax.all_to_all(values, "sp", split_axis=2, concat_axis=1, tiled=True),
    )
    seqs = query_all.shape[0]
    length = query_all.shape[1]
    first_head = lax.axis_index("sp") * heads_here
    ratios = lax.dynamic_slice_in_dim(mix_ratio, first_head, heads_here, 0)
    item_ratios = jnp.tile(ratios, seqs)

    def by_item(field):
        return jnp.swapaxes(field, 1, 2).reshape(seqs * heads_here, length, field.shape[3])

    def one_head(head_items):
        query_head, key_head, value_head, ratio = head_items
        return head_attention(query_head, key_head, value_head, ratio, out_gain)

    heads = lax.map(
        one_head, (by_item(query_all), by_item(key_all), by_item(value_all), item_ratios)
    )
    attended = jnp.swapaxes(heads.reshape(seqs, heads_here, length, heads.shape[2]), 1, 2)
    returned = lax.all_to_all(attended, "sp", split_axis=1, concat_axis=2, tiled=True)
    tokens_here = returned.shape[1]
    token_rows = returned.reshape(seqs * tokens_here, -1)
    result = jnp.dot(
        token_rows,
        lax.all_gather(out_weight, "dp", axis=1, tiled=True),
        preferred_element_type=jnp.float32,
    ).astype(jnp.bfloat16)
    return result.reshape(seqs, tokens_here, -1)


def solution(mesh):
    in_specs = (
        P("dp", "sp", None, None),
        P("dp", "sp", None, None),
        P("dp", "sp", None, None),
        P(),
        P(),
        P(None, "dp"),
    )
    out_specs = P("dp", "sp", None)
    return jax.shard_map(
        on_device, mesh=mesh, in_specs=in_specs, out_specs=out_specs, check_vma=False
    )
```

profile of v0, /device:TPU:0, one launch (start us, length us, event | category | flops | bytes accessed | tf_op | source)
XLA Modules:
  0.0 221.7 jit_solution(10596133892505202635)
XLA Ops:
  6.5 2.2 %copy.37 = bf16[1,192,16,128]{3,1,0,2:T(8,128)(2,1)} copy(bf16[1,192,16,128]{3,2,1,0:T(8,128)(2,1)} %param.10) | data formatting | bytes 1572864 | tf_op args[0]
  8.8 4.2 %all-to-all-start = ((bf16[1,192,16,128]{3,1,0,2:T(8,128)(2,1)}), bf16[1,192,16,128]{3,1,0,2:T(8,128)(2,1)S(1)}, u32[]{:S(2)}, u32[]{:S(2)}) async-start(bf16[1,192,16,128]{3,1,0,2:T(8,128)(2,1)} %copy.37), calls=%async_computation | async-start | bytes 1572864 | tf_op jit(solution)/shard_map/all_to_all | solution.py:69
  13.0 2.2 %copy.40 = bf16[1,192,16,128]{3,1,0,2:T(8,128)(2,1)} copy(bf16[1,192,16,128]{3,2,1,0:T(8,128)(2,1)} %param.11) | data formatting | bytes 1572864 | tf_op args[1]
  15.2 9.3 %all-to-all-done = bf16[1,192,16,128]{3,1,0,2:T(8,128)(2,1)S(1)} async-done(((bf16[1,192,16,128]{3,1,0,2:T(8,128)(2,1)}), bf16[1,192,16,128]{3,1,0,2:T(8,128)(2,1)S(1)}, u32[]{:S(2)}, u32[]{:S(2)}) %all-to-all-start) | async-done | bytes 786464 | tf_op jit(solution)/shard_map/all_to_all | solution.py:69
  24.6 3.5 %all-to-all-start.1 = ((bf16[1,192,16,128]{3,1,0,2:T(8,128)(2,1)}), bf16[1,192,16,128]{3,1,0,2:T(8,128)(2,1)S(1)}, u32[]{:S(2)}, u32[]{:S(2)}) async-start(bf16[1,192,16,128]{3,1,0,2:T(8,128)(2,1)} %copy.40), calls=%async_computation.1 | async-start | bytes 1572864 | tf_op jit(solution)/shard_map/all_to_all | solution.py:70
  28.1 2.3 %copy.43 = bf16[1,192,16,128]{3,1,0,2:T(8,128)(2,1)} copy(bf16[1,192,16,128]{3,2,1,0:T(8,128)(2,1)} %param.12) | data formatting | bytes 1572864 | tf_op args[2]
  30.4 8.2 %all-to-all-done.1 = bf16[1,192,16,128]{3,1,0,2:T(8,128)(2,1)S(1)} async-done(((bf16[1,192,16,128]{3,1,0,2:T(8,128)(2,1)}), bf16[1,192,16,128]{3,1,0,2:T(8,128)(2,1)S(1)}, u32[]{:S(2)}, u32[]{:S(2)}) %all-to-all-start.1) | async-done | bytes 786464 | tf_op jit(solution)/shard_map/all_to_all | solution.py:70
  38.6 3.5 %all-to-all-start.2 = ((bf16[1,192,16,128]{3,1,0,2:T(8,128)(2,1)}), bf16[1,192,16,128]{3,1,0,2:T(8,128)(2,1)S(1)}, u32[]{:S(2)}, u32[]{:S(2)}) async-start(bf16[1,192,16,128]{3,1,0,2:T(8,128)(2,1)} %copy.43), calls=%async_computation.2 | async-start | bytes 1572864 | tf_op jit(solution)/shard_map/all_to_all | solution.py:71
  45.3 6.5 %all-to-all-done.2 = bf16[1,192,16,128]{3,1,0,2:T(8,128)(2,1)S(1)} async-done(((bf16[1,192,16,128]{3,1,0,2:T(8,128)(2,1)}), bf16[1,192,16,128]{3,1,0,2:T(8,128)(2,1)S(1)}, u32[]{:S(2)}, u32[]{:S(2)}) %all-to-all-start.2) | async-done | bytes 786464 | tf_op jit(solution)/shard_map/all_to_all | solution.py:71
  51.8 143.6 %while.33 = (s32[]{:T(128)}, bf16[8,384,128]{2,1,0:T(8,128)(2,1)}, bf16[8,384,128]{1,2,0:T(8,128)(2,1)S(1)}, bf16[8,384,128]{1,2,0:T(8,128)(2,1)S(1)}, f32[8]{0:...) while((s32[]{:T(128)}, bf16[8,384,128]{2,1,0:T(8,128)(2,1)}, ...), condition=%wide.region_8.9_spmd, body=%wide.region_0.8_spmd.sunk | while | flops 26882248 | bytes 4764884 | solution.py:86
  53.1 16.0 %while.34 = (s32[]{:T(128)}, bf16[3,128,128]{2,1,0:T(8,128)(2,1)S(1)}, s32[3]{0:T(128)S(1)}, bf16[384,128]{0,1:T(8,128)(2,1)S(1)}, bf16[384,128]{1,0:T(8,128)(2,...) while((s32[]{:T(128)}, ...), condition=%wide.region_7.7_spmd.clone, body=%wide.region_1.6_spmd.clone.sunk | while | flops 26083076 | bytes 1811655 | solution.py:62
  62.6 0.9 multiply_reduce_fusion.2
  67.9 0.9 multiply_reduce_fusion.2
  71.1 16.0 %while.34 = (s32[]{:T(128)}, bf16[3,128,128]{2,1,0:T(8,128)(2,1)S(1)}, s32[3]{0:T(128)S(1)}, bf16[384,128]{0,1:T(8,128)(2,1)S(1)}, bf16[384,128]{1,0:T(8,128)(2,...) while((s32[]{:T(128)}, ...), condition=%wide.region_7.7_spmd.clone, body=%wide.region_1.6_spmd.clone.sunk | while | flops 26083076 | bytes 1811655 | solution.py:62
  85.9 0.9 multiply_reduce_fusion.2
  89.0 16.0 %while.34 = (s32[]{:T(128)}, bf16[3,128,128]{2,1,0:T(8,128)(2,1)S(1)}, s32[3]{0:T(128)S(1)}, bf16[384,128]{0,1:T(8,128)(2,1)S(1)}, bf16[384,128]{1,0:T(8,128)(2,...) while((s32[]{:T(128)}, ...), condition=%wide.region_7.7_spmd.clone, body=%wide.region_1.6_spmd.clone.sunk | while | flops 26083076 | bytes 1811655 | solution.py:62
  93.1 0.9 multiply_reduce_fusion.2
  98.5 0.9 multiply_reduce_fusion.2
  103.8 0.9 multiply_reduce_fusion.2
  107.0 16.0 %while.34 = (s32[]{:T(128)}, bf16[3,128,128]{2,1,0:T(8,128)(2,1)S(1)}, s32[3]{0:T(128)S(1)}, bf16[384,128]{0,1:T(8,128)(2,1)S(1)}, bf16[384,128]{1,0:T(8,128)(2,...) while((s32[]{:T(128)}, ...), condition=%wide.region_7.7_spmd.clone, body=%wide.region_1.6_spmd.clone.sunk | while | flops 26083076 | bytes 1811655 | solution.py:62
  121.8 1.0 multiply_reduce_fusion.2
  124.9 16.0 %while.34 = (s32[]{:T(128)}, bf16[3,128,128]{2,1,0:T(8,128)(2,1)S(1)}, s32[3]{0:T(128)S(1)}, bf16[384,128]{0,1:T(8,128)(2,1)S(1)}, bf16[384,128]{1,0:T(8,128)(2,...) while((s32[]{:T(128)}, ...), condition=%wide.region_7.7_spmd.clone, body=%wide.region_1.6_spmd.clone.sunk | while | flops 26083076 | bytes 1811655 | solution.py:62
  129.0 0.9 multiply_reduce_fusion.2
  142.8 16.0 %while.34 = (s32[]{:T(128)}, bf16[3,128,128]{2,1,0:T(8,128)(2,1)S(1)}, s32[3]{0:T(128)S(1)}, bf16[384,128]{0,1:T(8,128)(2,1)S(1)}, bf16[384,128]{1,0:T(8,128)(2,...) while((s32[]{:T(128)}, ...), condition=%wide.region_7.7_spmd.clone, body=%wide.region_1.6_spmd.clone.sunk | while | flops 26083076 | bytes 1811655 | solution.py:62
  147.0 0.9 multiply_reduce_fusion.2
  160.8 16.0 %while.34 = (s32[]{:T(128)}, bf16[3,128,128]{2,1,0:T(8,128)(2,1)S(1)}, s32[3]{0:T(128)S(1)}, bf16[384,128]{0,1:T(8,128)(2,1)S(1)}, bf16[384,128]{1,0:T(8,128)(2,...) while((s32[]{:T(128)}, ...), condition=%wide.region_7.7_spmd.clone, body=%wide.region_1.6_spmd.clone.sunk | while | flops 26083076 | bytes 1811655 | solution.py:62
  164.9 0.9 multiply_reduce_fusion.2
  178.7 16.0 %while.34 = (s32[]{:T(128)}, bf16[3,128,128]{2,1,0:T(8,128)(2,1)S(1)}, s32[3]{0:T(128)S(1)}, bf16[384,128]{0,1:T(8,128)(2,1)S(1)}, bf16[384,128]{1,0:T(8,128)(2,...) while((s32[]{:T(128)}, ...), condition=%wide.region_7.7_spmd.clone, body=%wide.region_1.6_spmd.clone.sunk | while | flops 26083076 | bytes 1811655 | solution.py:62
  182.9 0.9 multiply_reduce_fusion.2
  195.4 1.6 copy.59
  197.1 11.2 %all_to_all.69 = bf16[1,384,8,128]{3,2,0,1:T(8,128)(2,1)S(1)} all-to-all(bf16[1,384,8,128]{3,2,0,1:T(8,128)(2,1)S(1)} %bitcast.88), channel_id=1, replica_groups=mesh['sp'=2,'dp'=16] {'sp'}, dimensions={1} | all-to-all | bytes 1572864 | tf_op jit(solution)/shard_map/all_to_all | solution.py:90
  208.8 6.1 %fusion.12 = bf16[1,192,2048]{2,1,0:T(8,128)(2,1)} fusion(bf16[192,2048]{1,0:T(8,128)(2,1)S(1)} %reshape.130, bf16[2048,2048]{1,0:T(8,128)(2,1)} %all-gather.2.cloned.1.call-done), kind=kOutput, calls=%fused_computation.38 | convolution fusion | flops 1611005952 | bytes 9961472 | tf_op jit(solution)/shard_map/dot_general | solution.py:93
  (367 shorter events, 89.4 us)
Async XLA Ops:
  6.5 36.4 %copy-start.1 = (f32[16]{0:T(128)S(1)}, f32[16]{0:T(128)}, u32[]{:S(2)}) copy-start(f32[16]{0:T(128)} %param.13) | copy-start | bytes 196
  8.8 15.8 %all-to-all-start = ((bf16[1,192,16,128]{3,1,0,2:T(8,128)(2,1)}), bf16[1,192,16,128]{3,1,0,2:T(8,128)(2,1)S(1)}, u32[]{:S(2)}, u32[]{:S(2)}) async-start(bf16[1,192,16,128]{3,1,0,2:T(8,128)(2,1)} %copy.37), calls=%async_computation | async-start | bytes 1572864 | tf_op jit(solution)/shard_map/all_to_all | solution.py:69
  15.2 36.6 %copy-start = (f32[128]{0:T(128)S(1)}, f32[128]{0:T(128)}, u32[]{:S(2)}) copy-start(f32[128]{0:T(128)} %param.14) | copy-start | bytes 1540
  24.6 14.0 %all-to-all-start.1 = ((bf16[1,192,16,128]{3,1,0,2:T(8,128)(2,1)}), bf16[1,192,16,128]{3,1,0,2:T(8,128)(2,1)S(1)}, u32[]{:S(2)}, u32[]{:S(2)}) async-start(bf16[1,192,16,128]{3,1,0,2:T(8,128)(2,1)} %copy.40), calls=%async_computation.1 | async-start | bytes 1572864 | tf_op jit(solution)/shard_map/all_to_all | solution.py:70
  38.6 13.2 %all-to-all-start.2 = ((bf16[1,192,16,128]{3,1,0,2:T(8,128)(2,1)}), bf16[1,192,16,128]{3,1,0,2:T(8,128)(2,1)S(1)}, u32[]{:S(2)}, u32[]{:S(2)}) async-start(bf16[1,192,16,128]{3,1,0,2:T(8,128)(2,1)} %copy.43), calls=%async_computation.2 | async-start | bytes 1572864 | tf_op jit(solution)/shard_map/all_to_all | solution.py:71
  42.1 166.6 %all-gather.2.cloned.1.call-start = ((), (), s32[]{:S(2)}) async-start(), calls=%async_computation.4 | async-start | bytes 8912896 | tf_op jit(solution)/shard_map/all_gather | solution.py:95
Sparse Core Ops, SparseCore 0:
  45.1 79.5 all-gather.1
where the time goes:
time: 223 us; the launch traced here: 222 us
  loops' own time  47.4 us (21%)
  matrix products  47.1 us (21%)
  local copies, waits for them, and re-layouts  40.5 us (18%)
  other arithmetic  25.9 us (12%)
  waiting for transfers between devices  24.8 us (11%)
  between operations  13.5 us (6%)
  starting transfers between devices  11.3 us (5%)
  blocking collectives  11.2 us (5%)
    another operation x8, loops' own time, head_attention(): return lax.map(one_block, starts).reshape(length, value_head.shape[1])  46.7 us
    dot_general x24, matrix products, one_block(): mixed = jnp.dot(weights, value_head, preferred_element_type=jnp.float32)  22.8 us
    add x24, other arithmetic, one_block(): start + jnp.arange(block, dtype=jnp.int32)  15.2 us
    dynamic_slice x24, local copies, waits for them, and re-layouts, head_attention(): return lax.map(one_block, starts).reshape(length, value_head.shape[1])  14.6 us
    all_to_all x1, blocking collectives, on_device(): lax.all_to_all(attended, 'sp', split_axis=1, concat_axis=2, tiled=True)  11.2 us
    all_to_all x1, waiting for transfers between devices, on_device(): lax.all_to_all(queries, 'sp', split_axis=2, concat_axis=1, tiled=True)  9.35 us
    dot_general x24, matrix products, one_block(): jnp.dot(query_rows[:, width:], rotated_keys[:, width:].T, preferred_eleme...  9.13 us
    dot_general x24, matrix products, one_block(): jnp.dot(query_rows[:, :width], rotated_keys[:, :width].T, preferred_eleme...  9.12 us
  transfers between devices with their start and end apart: 4, of which 3 were waited for; matrix products, arithmetic and copies ran while one was open for 47% of the time, Pallas kernels for 0%

commit v1 on v0

--- a/solution.py
+++ b/solution.py
@@ -66,7 +66,10 @@
     groups = lax.axis_size("sp")
     heads_here = queries.shape[2] // groups
     query_all, key_all, value_all = (
-        lax.all_to_all(queries, "sp", split_axis=2, concat_axis=1, tiled=True),
+        jnp.concatenate(
+            lax.all_to_all(jnp.stack(jnp.split(queries, lax.axis_size("sp"), axis=2)), "sp", 0, 0),
+            axis=1,
+        ),
         lax.all_to_all(keys, "sp", split_axis=2, concat_axis=1, tiled=True),
         lax.all_to_all(values, "sp", split_axis=2, concat_axis=1, tiled=True),
     )

time: 223 us -> 230 us (1.031)
  local copies, waits for them, and re-layouts: 40.5 us -> 45.6 us
    dynamic_slice x16, local copies, waits for them, and re-layouts: 5.33 us -> 12.6 us  [on_device(): lax.map(one_head, (by_item(query_all), by_item(key_all), by_item(value_al...]
    unnamed x7 -> x8, local copies, waits for them, and re-layouts: 6.74 us -> 3.3 us
  transfers between devices with their start and end apart: 4 -> 4, of which waited for: 3 -> 3; matrix products, arithmetic and copies ran while one was open for 47% -> 49% of each run, Pallas kernels for 0% -> 0%
where the time goes in v1:
time: 230 us; the launch traced here: 229 us
  matrix products  48.4 us (21%)
  loops' own time  46.3 us (20%)
  local copies, waits for them, and re-layouts  45.6 us (20%)
  other arithmetic  26.6 us (12%)
  waiting for transfers between devices  25.7 us (11%)
  between operations  13.5 us (6%)
  starting transfers between devices  11.5 us (5%)
  blocking collectives  11.2 us (5%)
    another operation x8, loops' own time, head_attention(): return lax.map(one_block, starts).reshape(length, value_head.shape[1])  45.6 us
    dot_general x24, matrix products, one_block(): mixed = jnp.dot(weights, value_head, preferred_element_type=jnp.float32)  24.1 us
    add x24, other arithmetic, one_block(): start + jnp.arange(block, dtype=jnp.int32)  14.9 us
    dynamic_slice x24, local copies, waits for them, and re-layouts, head_attention(): return lax.map(one_block, starts).reshape(length, value_head.shape[1])  14.3 us
    dynamic_slice x16, local copies, waits for them, and re-layouts, on_device(): lax.map(one_head, (by_item(query_all), by_item(key_all), by_item(value_al...  12.6 us
    all_to_all x1, blocking collectives, on_device(): lax.all_to_all(attended, 'sp', split_axis=1, concat_axis=2, tiled=True)  11.2 us
    all_to_all x1, waiting for transfers between devices, on_device(): lax.all_to_all(keys, 'sp', split_axis=2, concat_axis=1, tiled=True)  9.39 us
    all_to_all x1, waiting for transfers between devices, on_device(): lax.all_to_all(jnp.stack(jnp.split(queries, lax.axis_size('sp'), axis=2))...  9.36 us
  transfers between devices with their start and end apart: 4, of which 3 were waited for; matrix products, arithmetic and copies ran while one was open for 49% of the time, Pallas kernels for 0%

profile of v1, /device:TPU:0, one launch (start us, length us, event | category | flops | bytes accessed | tf_op | source)
XLA Modules:
  0.0 228.7 jit_solution(8788406123953936512)
XLA Ops:
  6.5 1.2 slice_bitcast_fusion.1
  8.7 4.4 %all-to-all-start = ((bf16[2,1,192,8,128]{4,3,2,1,0:T(8,128)(2,1)}), bf16[2,1,192,8,128]{4,3,2,1,0:T(8,128)(2,1)S(1)}, u32[]{:S(2)}, u32[]{:S(2)}) async-start(bf16[2,1,192,8,128]{4,3,2,1,0:T(8,128)(2,1)} %pad_maximum_fusion.1), calls=%async_computation | async-start | bytes 1572864 | tf_op jit(solution)/shard_map/all_to_all | solution.py:70
  13.1 2.2 copy.36
  15.3 9.4 %all-to-all-done = bf16[2,1,192,8,128]{4,3,2,1,0:T(8,128)(2,1)S(1)} async-done(((bf16[2,1,192,8,128]{4,3,2,1,0:T(8,128)(2,1)}), bf16[2,1,192,8,128]{4,3,2,1,0:T(8,128)(2,1)S(1)}, u32[]{:S(2)}, u32[]{:S(2)}) %all-to-all-start) | async-done | bytes 786464 | tf_op jit(solution)/shard_map/all_to_all | solution.py:70
  24.7 3.5 %all-to-all-start.1 = ((bf16[1,192,16,128]{3,1,0,2:T(8,128)(2,1)}), bf16[1,192,16,128]{3,1,0,2:T(8,128)(2,1)S(1)}, u32[]{:S(2)}, u32[]{:S(2)}) async-start(bf16[1,192,16,128]{3,1,0,2:T(8,128)(2,1)} %copy.36), calls=%async_computation.1 | async-start | bytes 1572864 | tf_op jit(solution)/shard_map/all_to_all | solution.py:73
  28.2 1.1 copy.39
  29.3 9.4 %all-to-all-done.1 = bf16[1,192,16,128]{3,1,0,2:T(8,128)(2,1)S(1)} async-done(((bf16[1,192,16,128]{3,1,0,2:T(8,128)(2,1)}), bf16[1,192,16,128]{3,1,0,2:T(8,128)(2,1)S(1)}, u32[]{:S(2)}, u32[]{:S(2)}) %all-to-all-start.1) | async-done | bytes 786464 | tf_op jit(solution)/shard_map/all_to_all | solution.py:73
  38.7 3.5 %all-to-all-start.2 = ((bf16[1,192,16,128]{3,1,0,2:T(8,128)(2,1)}), bf16[1,192,16,128]{3,1,0,2:T(8,128)(2,1)S(1)}, u32[]{:S(2)}, u32[]{:S(2)}) async-start(bf16[1,192,16,128]{3,1,0,2:T(8,128)(2,1)} %copy.39), calls=%async_computation.2 | async-start | bytes 1572864 | tf_op jit(solution)/shard_map/all_to_all | solution.py:74
  44.2 1.4 copy.42
  45.7 6.2 %all-to-all-done.2 = bf16[1,192,16,128]{3,1,0,2:T(8,128)(2,1)S(1)} async-done(((bf16[1,192,16,128]{3,1,0,2:T(8,128)(2,1)}), bf16[1,192,16,128]{3,1,0,2:T(8,128)(2,1)S(1)}, u32[]{:S(2)}, u32[]{:S(2)}) %all-to-all-start.2) | async-done | bytes 786464 | tf_op jit(solution)/shard_map/all_to_all | solution.py:74
  51.9 150.5 %while.33 = (s32[]{:T(128)}, bf16[8,384,128]{2,1,0:T(8,128)(2,1)}, bf16[8,384,128]{1,2,0:T(8,128)(2,1)S(1)}, bf16[8,384,128]{1,2,0:T(8,128)(2,1)}, f32[8]{0:T(12...) while((s32[]{:T(128)}, bf16[8,384,128]{2,1,0:T(8,128)(2,1)}, ...), condition=%wide.region_8.9_spmd, body=%wide.region_0.8_spmd.sunk | while | flops 26882248 | bytes 4764884 | solution.py:89
  54.1 16.0 %while.34 = (s32[]{:T(128)}, bf16[3,128,128]{2,1,0:T(8,128)(2,1)S(1)}, s32[3]{0:T(128)S(1)}, bf16[384,128]{0,1:T(8,128)(2,1)S(1)}, bf16[384,128]{1,0:T(8,128)(2,...) while((s32[]{:T(128)}, ...), condition=%wide.region_7.7_spmd.clone, body=%wide.region_1.6_spmd.clone.sunk | while | flops 26083076 | bytes 1811655 | solution.py:62
  58.2 1.0 multiply_reduce_fusion.2
  63.5 1.0 multiply_reduce_fusion.2
  68.8 1.0 multiply_reduce_fusion.2
  72.9 16.0 %while.34 = (s32[]{:T(128)}, bf16[3,128,128]{2,1,0:T(8,128)(2,1)S(1)}, s32[3]{0:T(128)S(1)}, bf16[384,128]{0,1:T(8,128)(2,1)S(1)}, bf16[384,128]{1,0:T(8,128)(2,...) while((s32[]{:T(128)}, ...), condition=%wide.region_7.7_spmd.clone, body=%wide.region_1.6_spmd.clone.sunk | while | flops 26083076 | bytes 1811655 | solution.py:62
  77.0 1.0 multiply_reduce_fusion.2
  82.3 1.0 multiply_reduce_fusion.2
  87.6 1.0 multiply_reduce_fusion.2
  91.7 16.0 %while.34 = (s32[]{:T(128)}, bf16[3,128,128]{2,1,0:T(8,128)(2,1)S(1)}, s32[3]{0:T(128)S(1)}, bf16[384,128]{0,1:T(8,128)(2,1)S(1)}, bf16[384,128]{1,0:T(8,128)(2,...) while((s32[]{:T(128)}, ...), condition=%wide.region_7.7_spmd.clone, body=%wide.region_1.6_spmd.clone.sunk | while | flops 26083076 | bytes 1811655 | solution.py:62
  95.8 1.0 multiply_reduce_fusion.2
  101.1 1.0 multiply_reduce_fusion.2
  110.5 16.0 %while.34 = (s32[]{:T(128)}, bf16[3,128,128]{2,1,0:T(8,128)(2,1)S(1)}, s32[3]{0:T(128)S(1)}, bf16[384,128]{0,1:T(8,128)(2,1)S(1)}, bf16[384,128]{1,0:T(8,128)(2,...) while((s32[]{:T(128)}, ...), condition=%wide.region_7.7_spmd.clone, body=%wide.region_1.6_spmd.clone.sunk | while | flops 26083076 | bytes 1811655 | solution.py:62
  114.6 1.0 multiply_reduce_fusion.2
  119.9 1.0 multiply_reduce_fusion.2
  129.3 16.0 %while.34 = (s32[]{:T(128)}, bf16[3,128,128]{2,1,0:T(8,128)(2,1)S(1)}, s32[3]{0:T(128)S(1)}, bf16[384,128]{0,1:T(8,128)(2,1)S(1)}, bf16[384,128]{1,0:T(8,128)(2,...) while((s32[]{:T(128)}, ...), condition=%wide.region_7.7_spmd.clone, body=%wide.region_1.6_spmd.clone.sunk | while | flops 26083076 | bytes 1811655 | solution.py:62
  148.1 16.0 %while.34 = (s32[]{:T(128)}, bf16[3,128,128]{2,1,0:T(8,128)(2,1)S(1)}, s32[3]{0:T(128)S(1)}, bf16[384,128]{0,1:T(8,128)(2,1)S(1)}, bf16[384,128]{1,0:T(8,128)(2,...) while((s32[]{:T(128)}, ...), condition=%wide.region_7.7_spmd.clone, body=%wide.region_1.6_spmd.clone.sunk | while | flops 26083076 | bytes 1811655 | solution.py:62
  166.9 16.0 %while.34 = (s32[]{:T(128)}, bf16[3,128,128]{2,1,0:T(8,128)(2,1)S(1)}, s32[3]{0:T(128)S(1)}, bf16[384,128]{0,1:T(8,128)(2,1)S(1)}, bf16[384,128]{1,0:T(8,128)(2,...) while((s32[]{:T(128)}, ...), condition=%wide.region_7.7_spmd.clone, body=%wide.region_1.6_spmd.clone.sunk | while | flops 26083076 | bytes 1811655 | solution.py:62
  185.8 16.0 %while.34 = (s32[]{:T(128)}, bf16[3,128,128]{2,1,0:T(8,128)(2,1)S(1)}, s32[3]{0:T(128)S(1)}, bf16[384,128]{0,1:T(8,128)(2,1)S(1)}, bf16[384,128]{1,0:T(8,128)(2,...) while((s32[]{:T(128)}, ...), condition=%wide.region_7.7_spmd.clone, body=%wide.region_1.6_spmd.clone.sunk | while | flops 26083076 | bytes 1811655 | solution.py:62
  202.4 1.6 copy.54
  204.0 11.2 %all_to_all.56 = bf16[1,384,8,128]{3,2,0,1:T(8,128)(2,1)S(1)} all-to-all(bf16[1,384,8,128]{3,2,0,1:T(8,128)(2,1)S(1)} %bitcast.86), channel_id=1, replica_groups=mesh['sp'=2,'dp'=16] {'sp'}, dimensions={1} | all-to-all | bytes 1572864 | tf_op jit(solution)/shard_map/all_to_all | solution.py:93
  215.8 6.1 %fusion.12 = bf16[1,192,2048]{2,1,0:T(8,128)(2,1)} fusion(bf16[192,2048]{1,0:T(8,128)(2,1)S(1)} %reshape.134, bf16[2048,2048]{1,0:T(8,128)(2,1)} %all-gather.2.cloned.1.call-done), kind=kOutput, calls=%fused_computation.38 | convolution fusion | flops 1611005952 | bytes 9961472 | tf_op jit(solution)/shard_map/dot_general | solution.py:96
  (368 shorter events, 97.6 us)
Async XLA Ops:
  6.5 21.7 %copy-start = (bf16[1,192,16,128]{3,2,1,0:T(8,128)(2,1)S(1)}, bf16[1,192,16,128]{3,2,1,0:T(8,128)(2,1)}, u32[]{:S(2)}) copy-start(bf16[1,192,16,128]{3,2,1,0:T(8,128)(2,1)} %param.12) | copy-start | bytes 2359300
  6.5 36.5 %copy-start.2 = (f32[16]{0:T(128)S(1)}, f32[16]{0:T(128)}, u32[]{:S(2)}) copy-start(f32[16]{0:T(128)} %param.13) | copy-start | bytes 196
  8.7 43.2 %copy-start.1 = (f32[128]{0:T(128)S(1)}, f32[128]{0:T(128)}, u32[]{:S(2)}) copy-start(f32[128]{0:T(128)} %param.14) | copy-start | bytes 1540
  8.7 15.9 %all-to-all-start = ((bf16[2,1,192,8,128]{4,3,2,1,0:T(8,128)(2,1)}), bf16[2,1,192,8,128]{4,3,2,1,0:T(8,128)(2,1)S(1)}, u32[]{:S(2)}, u32[]{:S(2)}) async-start(bf16[2,1,192,8,128]{4,3,2,1,0:T(8,128)(2,1)} %pad_maximum_fusion.1), calls=%async_computation | async-start | bytes 1572864 | tf_op jit(solution)/shard_map/all_to_all | solution.py:70
  24.7 14.0 %all-to-all-start.1 = ((bf16[1,192,16,128]{3,1,0,2:T(8,128)(2,1)}), bf16[1,192,16,128]{3,1,0,2:T(8,128)(2,1)S(1)}, u32[]{:S(2)}, u32[]{:S(2)}) async-start(bf16[1,192,16,128]{3,1,0,2:T(8,128)(2,1)} %copy.36), calls=%async_computation.1 | async-start | bytes 1572864 | tf_op jit(solution)/shard_map/all_to_all | solution.py:73
  38.7 13.2 %all-to-all-start.2 = ((bf16[1,192,16,128]{3,1,0,2:T(8,128)(2,1)}), bf16[1,192,16,128]{3,1,0,2:T(8,128)(2,1)S(1)}, u32[]{:S(2)}, u32[]{:S(2)}) async-start(bf16[1,192,16,128]{3,1,0,2:T(8,128)(2,1)} %copy.39), calls=%async_computation.2 | async-start | bytes 1572864 | tf_op jit(solution)/shard_map/all_to_all | solution.py:74
  42.2 173.5 %all-gather.2.cloned.1.call-start = ((), (), s32[]{:S(2)}) async-start(), calls=%async_computation.4 | async-start | bytes 8912896 | tf_op jit(solution)/shard_map/all_gather | solution.py:98
Sparse Core Ops, SparseCore 0:
  45.2 79.3 all-gather.1
